TPU v7x, 128 devices: a whole 4x4x4 slice. The times are simulated.
128 devices in a mesh: rep: 2 (over z_hi), fs: 32 (over z_lo, y, x), tp: 2 (over core).
Axes of the slice: x: 4, y: 4, z: 4 (z_hi: 2, z_lo: 2; z = z_hi * 2 + z_lo), core: 2. Of those that a mesh axis runs over, the one named last changes fastest.
Arguments:
- tokens: bfloat16 [65536, 2048], P(('rep', 'fs', 'tp')), parts along dimension 0, may hold values from -6 to 6
- mix_gain: float32 [2048], replicated, may hold values from 0.1 to 1.9
- w_query: bfloat16 [2048, 512], P('fs', 'tp'), may hold values from -0.125 to 0.125
- w_key: bfloat16 [2048, 512], P('fs', 'tp'), may hold values from -0.125 to 0.125
- w_value: bfloat16 [2048, 1024], P('fs', 'tp'), may hold values from -0.125 to 0.125
- w_out: bfloat16 [1024, 2048], P('tp', 'fs'), may hold values from -0.1875 to 0.1875
- ffn_gain: float32 [2048], replicated, may hold values from 0.1 to 1.9
- w_ffgate: bfloat16 [2048, 2816], P('fs', 'tp'), may hold values from -0.125 to 0.125
- w_ffup: bfloat16 [2048, 2816], P('fs', 'tp'), may hold values from -0.125 to 0.125
- conv_gate: float32 [3, 2816], replicated, may hold values from -3 to 3
- conv_up: float32 [3, 2816], replicated, may hold values from -3 to 3
- w_down: bfloat16 [2816, 2048], P('tp', 'fs'), may hold values from -0.109375 to 0.109375
Outputs:
- layer_out: bfloat16 [65536, 2048], P(('rep', 'fs', 'tp')), parts along dimension 0
There are 2 independent parts, one for each index of `rep`. A program takes and returns all parts, laid end to end along the dimension named above; an argument that names none is the same for every part. Nothing has to cross between parts.
All inputs are finite; a program needn't handle non-finite values.
Results may differ from a plain program's by a relative error of at most 0.014.
Values may be sent and summed in bfloat16 or wider, within the bound.
No kernel may reach another device: no remote copies, remote signals or barrier semaphores. Data moves between devices by JAX's collectives and lax.ppermute only.
A program may use at most 128 MiB of HBM per device.

v0:
```python
import jax
import jax.numpy as jnp
from jax import lax
from jax.sharding import PartitionSpec as P

HEADS = 4
DK = 128
DV = 256
KERNEL = 3
BLOCK = 128
LENGTH = 1024
epsilon = 1e-06


def in_one_piece(arrays, axis, dim, along):
    both = jnp.concatenate(arrays, axis=along)
    out, at, done = (lax.all_gather(both, axis, axis=dim, tiled=True), 0, [])
    for a in arrays:
        done.append(lax.slice_in_dim(out, at, at + a.shape[along], axis=along))
        at += a.shape[along]
    return tuple(done)


def copy_for_each(shard, axis):
    length = lax.axis_size(axis)
    return lax.all_to_all(
        jnp.broadcast_to(shard[None], (length, *shard.shape)), axis, 0, 0, tiled=True
    )


def in_order(pieces, dim):
    pieces = jnp.moveaxis(pieces, 0, dim)
    dims = pieces.shape
    return pieces.reshape(*dims[:dim], dims[dim] * dims[dim + 1], *dims[dim + 2 :])


def collect(shard, axis, dim):
    pieces = copy_for_each(shard, axis)
    return in_order(pieces, dim)


def in_blocks(shard, dim, length):
    dims = shard.shape
    pieces = shard.reshape(*dims[:dim], length, dims[dim] // length, *dims[dim + 1 :])
    return jnp.moveaxis(pieces, dim, 0)


def sent_and_summed(shard, axis, dim):
    length = lax.axis_size(axis)
    pieces = lax.all_to_all(in_blocks(shard, dim, length), axis, 0, 0, tiled=True)
    return jnp.sum(pieces.astype(jnp.float32), axis=0)


def rms_rows(matrix, scale_vec):
    values = matrix.astype(jnp.float32)
    factor = lax.rsqrt(jnp.mean(values * values, axis=-1, keepdims=True) + epsilon)
    return (values * factor * scale_vec).astype(jnp.bfloat16)


def rotate_heads(matrix):
    length = matrix.shape[0]
    half_width = matrix.shape[-1] // 2
    inverse = 10000.0 ** (-jnp.arange(half_width, dtype=jnp.float32) * 2.0 / (2 * half_width))
    angles = jnp.arange(length, dtype=jnp.float32)[:, None] * inverse[None, :]
    cosine = jnp.cos(angles)[:, None, :]
    sine = jnp.sin(angles)[:, None, :]
    values = matrix.astype(jnp.float32)
    first_half = values[..., :half_width]
    second_half = values[..., half_width:]
    return jnp.concatenate(
        [first_half * cosine - second_half * sine, first_half * sine + second_half * cosine],
        axis=-1,
    )


def retain_blocks(rot_query, rot_key, value, rates, block_len):
    length, head_count, width_k = rot_query.shape
    width_v = value.shape[-1]
    blocks = length // block_len
    query4 = rot_query.reshape(blocks, block_len, head_count, width_k)
    key4 = rot_key.reshape(blocks, block_len, head_count, width_k)
    value4 = value.reshape(blocks, block_len, head_count, width_v)
    places = jnp.arange(block_len, dtype=jnp.float32)
    spacing = places[:, None] - places[None, :]
    inside = jnp.where(
        spacing[None] >= 0, jnp.exp(-jnp.maximum(spacing, 0.0)[None] * rates[:, None, None]), 0.0
    )
    scores = jnp.einsum("cihd,cjhd->chij", query4, key4, preferred_element_type=jnp.float32)
    weights = (scores * inside[None]).astype(jnp.bfloat16)
    inner_part = jnp.einsum("chij,cjhe->cihe", weights, value4, preferred_element_type=jnp.float32)
    tail_decay = jnp.exp(-(block_len - 1.0 - places)[:, None] * rates[None, :])
    decayed = (key4.astype(jnp.float32) * tail_decay[None, :, :, None]).astype(jnp.bfloat16)
    states = jnp.einsum("cjhd,cjhe->chde", decayed, value4, preferred_element_type=jnp.float32)
    passing = jnp.exp(-block_len * rates)[:, None, None]

    def advance(carried, fresh):
        return (carried * passing + fresh, carried)

    _, before = lax.scan(advance, jnp.zeros((head_count, width_k, width_v), jnp.float32), states)
    onset_decay = jnp.exp(-(places + 1.0)[:, None] * rates[None, :])
    cross_part = (
        jnp.einsum("cihd,chde->cihe", query4.astype(jnp.float32), before)
        * onset_decay[None, :, :, None]
    )
    return (inner_part + cross_part).reshape(length, head_count, width_v)


def head_norm(retained):
    average = jnp.mean(retained, axis=-1, keepdims=True)
    centered = retained - average
    return centered * lax.rsqrt(jnp.mean(centered * centered, axis=-1, keepdims=True) + epsilon)


def causal_taps(matrix, kernel_w):
    length = matrix.shape[0]
    padded = jnp.pad(matrix.astype(jnp.float32), ((KERNEL - 1, 0), (0, 0)))
    total = jnp.zeros((length, matrix.shape[1]), jnp.float32)
    for tap_idx in range(KERNEL):
        total = total + kernel_w[tap_idx][None, :] * padded[tap_idx : tap_idx + length]
    return total


def collect_ffn(w_ffgate, w_ffup):
    return in_one_piece((w_ffgate, w_ffup), "fs", 0, 1)


def body(
    tokens,
    mix_gain,
    w_query,
    w_key,
    w_value,
    w_out,
    ffn_gain,
    w_ffgate,
    w_ffup,
    conv_gate,
    conv_up,
    w_down,
):
    tp_rank = lax.axis_index("tp")
    heads_here = w_query.shape[1] // DK
    ffn_pair = None
    normed = rms_rows(tokens, mix_gain)
    query_w, key_w, value_w = in_one_piece((w_query, w_key, w_value), "fs", 0, 1)
    qk_cols = query_w.shape[1]
    pieces = lax.all_gather(normed, "tp", axis=0, tiled=True)
    joined = jnp.concatenate(
        [
            jnp.dot(pieces, query_w, preferred_element_type=jnp.float32),
            jnp.dot(pieces, key_w, preferred_element_type=jnp.float32),
            jnp.dot(pieces, value_w, preferred_element_type=jnp.float32),
        ],
        axis=1,
    ).astype(jnp.bfloat16)
    length = joined.shape[0]
    query = joined[:, :qk_cols].reshape(length, heads_here, DK)
    key = joined[:, qk_cols : 2 * qk_cols].reshape(length, heads_here, DK)
    value = joined[:, 2 * qk_cols :].reshape(length, heads_here, DV)
    rot_query = rotate_heads(query).astype(jnp.bfloat16)
    rot_key = (rotate_heads(key) * DK ** (-0.5)).astype(jnp.bfloat16)
    head_ids = (tp_rank * heads_here + jnp.arange(heads_here, dtype=jnp.int32)).astype(jnp.float32)
    rates = 1.0 / 16.0 * (32.0 / LENGTH) ** (head_ids / (HEADS - 1))
    retained = retain_blocks(rot_query, rot_key, value, rates, BLOCK)
    hidden = head_norm(retained).reshape(length, heads_here * DV).astype(jnp.bfloat16)
    out_full = collect(w_out, "fs", 1)
    mix_sum = sent_and_summed(
        jnp.dot(hidden, out_full, preferred_element_type=jnp.float32).astype(jnp.bfloat16), "tp", 0
    )
    resid = (tokens.astype(jnp.float32) + mix_sum).astype(jnp.bfloat16)
    normed_ffn = rms_rows(resid, ffn_gain)
    ff_here = w_ffgate.shape[1]
    ffn_pair = collect_ffn(w_ffgate, w_ffup)
    gate_w, up_w = ffn_pair
    pieces = lax.all_gather(normed_ffn, "tp", axis=0, tiled=True)
    both_pre = jnp.concatenate(
        [
            jnp.dot(pieces, gate_w, preferred_element_type=jnp.float32),
            jnp.dot(pieces, up_w, preferred_element_type=jnp.float32),
        ],
        axis=1,
    ).astype(jnp.bfloat16)
    gate_pre = both_pre[:, :ff_here]
    up_pre = both_pre[:, ff_here:]
    gate_taps = lax.dynamic_slice_in_dim(conv_gate, tp_rank * ff_here, ff_here, 1)
    up_taps = lax.dynamic_slice_in_dim(conv_up, tp_rank * ff_here, ff_here, 1)
    activ = (jax.nn.silu(causal_taps(gate_pre, gate_taps)) * causal_taps(up_pre, up_taps)).astype(
        jnp.bfloat16
    )
    down_full = lax.all_gather(w_down, "fs", axis=1, tiled=True)
    ffn_sum = sent_and_summed(
        jnp.dot(activ, down_full, preferred_element_type=jnp.float32).astype(jnp.bfloat16), "tp", 0
    )
    return (resid.astype(jnp.float32) + ffn_sum).astype(jnp.bfloat16)


def solution(mesh):
    placed = (
        P(("rep", "fs", "tp"), None),
        P(),
        P("fs", "tp"),
        P("fs", "tp"),
        P("fs", "tp"),
        P("tp", "fs"),
        P(),
        P("fs", "tp"),
        P("fs", "tp"),
        P(),
        P(),
        P("tp", "fs"),
    )
    return jax.shard_map(
        body, mesh=mesh, in_specs=placed, out_specs=P(("rep", "fs", "tp"), None), check_vma=False
    )
```

profile of v0, /device:TPU:1, one launch (start us, length us, event | category | flops | bytes accessed | tf_op | source)
XLA Modules:
  0.0 637.9 jit_solution(8390424234193751009)
XLA Ops:
  6.6 2.1 fusion.6
  8.7 3.5 fusion.8
  13.0 1.5 broadcast_in_dim.25
  14.5 9.3 %all-to-all-start = ((bf16[32,512,64]{1,2,0:T(8,128)(2,1)}), bf16[32,512,64]{1,2,0:T(8,128)(2,1)}, u32[]{:S(2)}, u32[]{:S(2)}) async-start(bf16[32,512,64]{1,2,0:T(8,128)(2,1)} %broadcast_in_dim.25), calls=%async_computation | async-start | bytes 4194304 | tf_op jit(solution)/shard_map/all_to_all | solution.py:26
  25.2 7.1 %all-gather.6.cloned.1.call-done = bf16[1024,2048]{1,0:T(8,128)(2,1)} async-done(((bf16[512,2048]{1,0:T(8,128)(2,1)}), bf16[1024,2048]{1,0:T(8,128)(2,1)}) %all-gather.6.cloned.1.call-update) | async-done | bytes 4194320 | tf_op jit(solution)/shard_map/all_gather | solution.py:147
  32.3 140.7 %all-gather.8.cloned.1.call-done = bf16[2048,1024]{1,0:T(8,128)(2,1)} async-done(((bf16[64,1024]{1,0:T(8,128)(2,1)}), bf16[2048,1024]{1,0:T(8,128)(2,1)}) %all-gather.8.cloned.1.call-update) | async-done | bytes 4194320 | tf_op jit(solution)/shard_map/all_gather | solution.py:17
  173.0 3.9 convolution_convert_fusion.3
  177.1 2.5 convolution_convert_fusion.2
  181.8 6.2 fusion.31
  187.9 1.3 reshape_reshape.3
  191.0 6.5 %while.13 = (s32[]{:T(128)}, f32[2,128,256]{2,1,0:T(8,128)S(1)}, bf16[8,2,128,256]{3,2,1,0:T(8,128)(2,1)}, f32[8,2,128,256]{3,2,1,0:T(8,128)S(1)}, s32[]{:T(128)}, /*index=5*/s32[]{:T(128)}, s32[]{:T(128)}) while((s32[]{:T(128)}, f32[2,128,256]{2,1,0:T(8,128)S(1)}, bf16[8,2,128,256]{3,2,1,0:T(8,128)(2,1)}, ...), condition=%wide.region_2.3_spmd.clone, body=%wide.region_1.2_spmd.clone.sunk | while | flops 262155 | bytes 1180272 | solution.py:99
  200.3 3.2 fusion.45
  203.6 3.0 fusion.54
  208.9 4.0 convolution_convert_fusion.1
  212.9 27.5 %all_to_all.15 = bf16[2,512,2048]{2,1,0:T(8,128)(2,1)S(1)} all-to-all(bf16[2,512,2048]{2,1,0:T(8,128)(2,1)S(1)} %bitcast.73), channel_id=1, replica_groups=mesh['rep'=2,'fs'=32,'tp'=2] {'tp'}, dimensions={0} | all-to-all | bytes 8388608 | tf_op jit(solution)/shard_map/all_to_all | solution.py:50
  242.7 1.9 fusion.12
  247.1 15.1 %all-gather.10.cloned.1.call-done = bf16[1024,2048]{1,0:T(8,128)(2,1)} async-done(((bf16[512,2048]{1,0:T(8,128)(2,1)}), bf16[1024,2048]{1,0:T(8,128)(2,1)}) %all-gather.10.cloned.1.call-update) | async-done | bytes 4194320 | tf_op jit(solution)/shard_map/all_gather | solution.py:175
  262.2 155.1 %all-gather.12.cloned.1.call-done = bf16[2048,2816]{1,0:T(8,128)(2,1)} async-done(((bf16[64,2816]{1,0:T(8,128)(2,1)}), bf16[2048,2816]{1,0:T(8,128)(2,1)}) %all-gather.12.cloned.1.call-update) | async-done | bytes 11534352 | tf_op jit(solution)/shard_map/all_gather | solution.py:17
  417.3 11.8 %fusion.17 = f32[1024,1408]{1,0:T(8,128)} fusion(bf16[1024,2048]{1,0:T(8,128)(2,1)} %all-gather.10.cloned.1.call-done, bf16[2048,2816]{1,0:T(8,128)(2,1)} %all-gather.12.cloned.1.call-done), kind=kOutput, calls=%fused_computation.26 | convolution fusion | flops 5908463616 | bytes 15728640 | tf_op jit(solution)/shard_map/dot_general | solution.py:178
  429.1 8.5 %fusion.23 = f32[1024,1408]{1,0:T(8,128)} fusion(bf16[1024,2048]{1,0:T(8,128)(2,1)S(1)} %copy-done.13, bf16[2048,2816]{1,0:T(8,128)(2,1)S(1)} %copy-done.11), kind=kOutput, calls=%fused_computation.28 | convolution fusion | flops 5908463616 | bytes 15728640 | tf_op jit(solution)/shard_map/dot_general | solution.py:179
  437.6 139.5 %all-gather.14.cloned.1.call-done = bf16[1408,2048]{0,1:T(8,128)(2,1)} async-done(((bf16[1408,64]{0,1:T(8,128)(2,1)}), bf16[1408,2048]{0,1:T(8,128)(2,1)}) %all-gather.14.cloned.1.call-update) | async-done | bytes 5767184 | tf_op jit(solution)/shard_map/all_gather | solution.py:190
  577.1 23.0 %convolution_convert_fusion = bf16[1024,2048]{1,0:T(8,128)(2,1)} fusion(bf16[1408,2048]{0,1:T(8,128)(2,1)} %all-gather.14.cloned.1.call-done, f32[1024,1408]{1,0:T(8,128)} %fusion.23, f32[1024,1408]{1,0:T(8,128)} %fusion.17, f32[1408]{0:T(1024)S(1)} %get-tuple-element.59, f32[1408]{0:T(1024)S(1)} %get-tuple-element.58, f32[1408]{0:T(1024)S(1)} %get-tuple-element.57, ...), kind=kOutput, calls=%fused_computation.29 | convolution fusion | flops 5930745856 | bytes 21529600 | tf_op jit(solution)/shard_map/dot_general | solution.py:192
  600.1 28.2 %all_to_all.16 = bf16[2,512,2048]{2,1,0:T(8,128)(2,1)S(1)} all-to-all(bf16[2,512,2048]{2,1,0:T(8,128)(2,1)} %bitcast.72), channel_id=1, replica_groups=mesh['rep'=2,'fs'=32,'tp'=2] {'tp'}, dimensions={0} | all-to-all | bytes 8388608 | tf_op jit(solution)/shard_map/all_to_all | solution.py:50
  629.3 2.1 fusion.13
  (100 shorter events, 23.1 us)
Async XLA Ops:
  6.5 5.7 copy-start.7
  6.5 5.7 copy-start.8
  6.5 5.7 copy-start.9
  6.5 6.4 %copy-start.6 = (bf16[512,64]{0,1:T(8,128)(2,1)S(1)}, bf16[512,64]{0,1:T(8,128)(2,1)}, u32[]{:S(2)}) copy-start(bf16[512,64]{0,1:T(8,128)(2,1)} %param.19) | copy-start | bytes 196612
  6.5 25.8 %all-gather.6.cloned.1.call-start = ((), (), s32[]{:S(2)}) async-start(), calls=%async_computation.3 | async-start | bytes 6291456 | tf_op jit(solution)/shard_map/all_gather | solution.py:147
  12.2 160.8 %all-gather.8.cloned.1.call-start = ((), (), s32[]{:S(2)}) async-start(), calls=%async_computation.4 | async-start | bytes 4325376 | tf_op jit(solution)/shard_map/all_gather | solution.py:17
  14.5 194.4 %all-to-all-start = ((bf16[32,512,64]{1,2,0:T(8,128)(2,1)}), bf16[32,512,64]{1,2,0:T(8,128)(2,1)}, u32[]{:S(2)}, u32[]{:S(2)}) async-start(bf16[32,512,64]{1,2,0:T(8,128)(2,1)} %broadcast_in_dim.25), calls=%async_computation | async-start | bytes 4194304 | tf_op jit(solution)/shard_map/all_to_all | solution.py:26
  23.9 238.3 %all-gather.10.cloned.1.call-start = ((), (), s32[]{:S(2)}) async-start(), calls=%async_computation.5 | async-start | bytes 6291456 | tf_op jit(solution)/shard_map/all_gather | solution.py:175
  173.0 4.1 copy-start.12
  189.6 0.8 copy-start.1
  198.8 4.8 copy-start.2
  200.3 3.2 copy-start.3
  240.4 1.6 copy-start
  241.9 0.7 copy-start.10
  242.6 2.0 copy-start.4
  242.6 2.0 copy-start.5
  244.6 172.7 %all-gather.12.cloned.1.call-start = ((), (), s32[]{:S(2)}) async-start(), calls=%async_computation.6 | async-start | bytes 11894784 | tf_op jit(solution)/shard_map/all_gather | solution.py:17
  245.4 331.7 %all-gather.14.cloned.1.call-start = ((), (), s32[]{:S(2)}) async-start(), calls=%async_computation.7 | async-start | bytes 5947392 | tf_op jit(solution)/shard_map/all_gather | solution.py:190
  417.3 11.8 %copy-start.11 = (bf16[2048,2816]{1,0:T(8,128)(2,1)S(1)}, bf16[2048,2816]{1,0:T(8,128)(2,1)}, u32[]{:S(2)}) copy-start(bf16[2048,2816]{1,0:T(8,128)(2,1)} %all-gather.12.cloned.1.call-done) | copy-start | bytes 34603012
  417.3 11.9 %copy-start.13 = (bf16[1024,2048]{1,0:T(8,128)(2,1)S(1)}, bf16[1024,2048]{1,0:T(8,128)(2,1)}, u32[]{:S(2)}) copy-start(bf16[1024,2048]{1,0:T(8,128)(2,1)} %all-gather.10.cloned.1.call-done) | copy-start | bytes 12582916
Sparse Core Ops, SparseCore 0:
  12.3 19.9 all-gather.5
  34.0 138.9 all-gather.7
  244.7 17.4 all-gather.9
  263.7 153.5 all-gather.11
  418.8 158.2 all-gather.13
where the time goes:
time: 639 us; the launch traced here: 638 us
  waiting for transfers between devices  458 us (72%)
  matrix products  66.7 us (10%)
  blocking collectives  55.7 us (9%)
  other arithmetic  24.3 us (4%)
  between operations  13.5 us (2%)
  local copies, waits for them, and re-layouts  9.83 us (2%)
  starting transfers between devices  9.54 us (1%)
    all_gather x2, waiting for transfers between devices, in_one_piece(): out, at, done = (lax.all_gather(both, axis, axis=dim, tiled=True), 0, [])  296 us
    all_gather x1, waiting for transfers between devices, body(): down_full = lax.all_gather(w_down, 'fs', axis=1, tiled=True)  139 us
    all_to_all x2, blocking collectives, sent_and_summed(): lax.all_to_all(in_blocks(shard, dim, length), axis, 0, 0, tiled=True)  55.7 us
    dot_general x1, matrix products, body(): jnp.dot(activ, down_full, preferred_element_type=jnp.float32)  23 us
    all_gather x1, waiting for transfers between devices, body(): pieces = lax.all_gather(normed_ffn, 'tp', axis=0, tiled=True)  15.1 us
  transfers between devices with their start and end apart: 6, of which 5 were waited for; matrix products, arithmetic and copies ran while one was open for 9% of the time, Pallas kernels for 0%

commit v1 on v0

--- a/solution.py
+++ b/solution.py
@@ -187,7 +187,7 @@
     activ = (jax.nn.silu(causal_taps(gate_pre, gate_taps)) * causal_taps(up_pre, up_taps)).astype(
         jnp.bfloat16
     )
-    down_full = lax.all_gather(w_down, "fs", axis=1, tiled=True)
+    down_full = jnp.concatenate(lax.all_gather(w_down, axis_name="fs"), axis=1)
     ffn_sum = sent_and_summed(
         jnp.dot(activ, down_full, preferred_element_type=jnp.float32).astype(jnp.bfloat16), "tp", 0
     )

time: 639 us -> 611 us (0.956)
  waiting for transfers between devices: 458 us -> 423 us
  local copies, waits for them, and re-layouts: 9.83 us -> 17.8 us
    all_gather x1, waiting for transfers between devices: 139 us -> 90.2 us  [body(): down_full = jnp.concatenate(lax.all_gather(w_down, axis_name='fs'), axis=1)]
    all_gather x1, waiting for transfers between devices: 15.1 us -> 30 us  [body(): pieces = lax.all_gather(normed_ffn, 'tp', axis=0, tiled=True)]
where the time goes in v1:
time: 611 us
  waiting for transfers between devices  423 us (69%)
  matrix products  66.8 us (11%)
  blocking collectives  55.6 us (9%)
  other arithmetic  24.4 us (4%)
  local copies, waits for them, and re-layouts  17.8 us (3%)
  between operations  13.6 us (2%)
  starting transfers between devices  9.76 us (2%)
    all_gather x2, waiting for transfers between devices, in_one_piece(): out, at, done = (lax.all_gather(both, axis, axis=dim, tiled=True), 0, [])  295 us
    all_gather x1, waiting for transfers between devices, body(): down_full = jnp.concatenate(lax.all_gather(w_down, axis_name='fs'), axis=1)  90.2 us
    all_to_all x2, blocking collectives, sent_and_summed(): lax.all_to_all(in_blocks(shard, dim, length), axis, 0, 0, tiled=True)  55.6 us
    all_gather x1, waiting for transfers between devices, body(): pieces = lax.all_gather(normed_ffn, 'tp', axis=0, tiled=True)  30 us
    dot_general x1, matrix products, body(): jnp.dot(activ, down_full, preferred_element_type=jnp.float32)  23 us
  transfers between devices with their start and end apart: 6, of which 5 were waited for; matrix products, arithmetic and copies ran while one was open for 9% of the time, Pallas kernels for 0%

profile of v1, /device:TPU:1, one launch (start us, length us, event | category | flops | bytes accessed | tf_op | source)
XLA Modules:
  0.0 610.7 jit_solution(13414776563466217259)
XLA Ops:
  6.6 2.1 fusion.6
  8.7 3.5 fusion.8
  14.6 9.3 %all-to-all-start = ((bf16[32,512,64]{1,2,0:T(8,128)(2,1)}), bf16[32,512,64]{1,2,0:T(8,128)(2,1)}, u32[]{:S(2)}, u32[]{:S(2)}) async-start(bf16[32,512,64]{1,2,0:T(8,128)(2,1)} %broadcast_in_dim.25), calls=%async_computation | async-start | bytes 4194304 | tf_op jit(solution)/shard_map/all_to_all | solution.py:26
  26.0 6.3 %all-gather.7.cloned.1.call-done = bf16[1024,2048]{1,0:T(8,128)(2,1)} async-done(((bf16[512,2048]{1,0:T(8,128)(2,1)}), bf16[1024,2048]{1,0:T(8,128)(2,1)}) %all-gather.7.cloned.1.call-update) | async-done | bytes 4194320 | tf_op jit(solution)/shard_map/all_gather | solution.py:147
  32.3 140.2 %all-gather.9.cloned.1.call-done = bf16[2048,1024]{1,0:T(8,128)(2,1)} async-done(((bf16[64,1024]{1,0:T(8,128)(2,1)}), bf16[2048,1024]{1,0:T(8,128)(2,1)}) %all-gather.9.cloned.1.call-update) | async-done | bytes 4194320 | tf_op jit(solution)/shard_map/all_gather | solution.py:17
  172.6 3.9 convolution_convert_fusion.3
  176.6 2.5 convolution_convert_fusion.2
  181.3 6.2 %fusion.31 = bf16[1024,512]{1,0:T(8,128)(2,1)} fusion(bf16[1024,2048]{1,0:T(8,128)(2,1)} %all-gather.7.cloned.1.call-done, bf16[2048,1024]{1,0:T(8,128)(2,1)} %all-gather.9.cloned.1.call-done), kind=kOutput, calls=%fused_computation.39 | convolution fusion | flops 2148007936 | bytes 7340032 | tf_op jit(solution)/shard_map/dot_general | solution.py:152
  190.5 6.5 %while.13 = (s32[]{:T(128)}, f32[2,128,256]{2,1,0:T(8,128)S(1)}, bf16[8,2,128,256]{3,2,1,0:T(8,128)(2,1)}, f32[8,2,128,256]{3,2,1,0:T(8,128)S(1)}, s32[]{:T(128)}, /*index=5*/s32[]{:T(128)}, s32[]{:T(128)}) while((s32[]{:T(128)}, f32[2,128,256]{2,1,0:T(8,128)S(1)}, bf16[8,2,128,256]{3,2,1,0:T(8,128)(2,1)}, ...), condition=%wide.region_2.3_spmd.clone, body=%wide.region_1.2_spmd.clone.sunk | while | flops 262155 | bytes 1180272 | solution.py:99
  199.9 3.2 fusion.45
  203.1 3.1 fusion.54
  208.5 4.0 convolution_convert_fusion.1
  212.5 27.4 %all_to_all.15 = bf16[2,512,2048]{2,1,0:T(8,128)(2,1)S(1)} all-to-all(bf16[2,512,2048]{2,1,0:T(8,128)(2,1)S(1)} %bitcast.83), channel_id=1, replica_groups=mesh['rep'=2,'fs'=32,'tp'=2] {'tp'}, dimensions={0} | all-to-all | bytes 8388608 | tf_op jit(solution)/shard_map/all_to_all | solution.py:50
  242.1 1.9 fusion.12
  246.2 90.2 %all-gather.15.cloned.1.call-done = bf16[45056,64]{0,1:T(8,128)(2,1)} async-done(((bf16[1408,64]{0,1:T(8,128)(2,1)}), bf16[45056,64]{0,1:T(8,128)(2,1)}) %all-gather.15.cloned.1.call-update) | async-done | bytes 5767184 | tf_op jit(solution)/shard_map/all_gather | solution.py:190
  336.4 3.5 copy.55
  340.0 4.4 copy.49
  344.4 30.0 %all-gather.11.cloned.1.call-done = bf16[1024,2048]{1,0:T(8,128)(2,1)} async-done(((bf16[512,2048]{1,0:T(8,128)(2,1)}), bf16[1024,2048]{1,0:T(8,128)(2,1)}) %all-gather.11.cloned.1.call-update) | async-done | bytes 4194320 | tf_op jit(solution)/shard_map/all_gather | solution.py:175
  374.5 155.1 %all-gather.13.cloned.1.call-done = bf16[2048,2816]{1,0:T(8,128)(2,1)} async-done(((bf16[64,2816]{1,0:T(8,128)(2,1)}), bf16[2048,2816]{1,0:T(8,128)(2,1)}) %all-gather.13.cloned.1.call-update) | async-done | bytes 11534352 | tf_op jit(solution)/shard_map/all_gather | solution.py:17
  529.6 11.8 %fusion.17 = f32[1024,1408]{1,0:T(8,128)} fusion(bf16[1024,2048]{1,0:T(8,128)(2,1)} %all-gather.11.cloned.1.call-done, bf16[2048,2816]{1,0:T(8,128)(2,1)} %all-gather.13.cloned.1.call-done), kind=kOutput, calls=%fused_computation.26 | convolution fusion | flops 5908463616 | bytes 15728640 | tf_op jit(solution)/shard_map/dot_general | solution.py:178
  541.4 8.5 %fusion.23 = f32[1024,1408]{1,0:T(8,128)} fusion(bf16[1024,2048]{1,0:T(8,128)(2,1)S(1)} %copy-done.13, bf16[2048,2816]{1,0:T(8,128)(2,1)S(1)} %copy-done.11), kind=kOutput, calls=%fused_computation.28 | convolution fusion | flops 5908463616 | bytes 15728640 | tf_op jit(solution)/shard_map/dot_general | solution.py:179
  549.9 23.0 %convolution_convert_fusion = bf16[1024,2048]{1,0:T(8,128)(2,1)} fusion(bf16[1408,2048]{0,1:T(8,128)(2,1)} %bitcast.81, f32[1024,1408]{1,0:T(8,128)} %fusion.23, f32[1024,1408]{1,0:T(8,128)} %fusion.17, f32[1408]{0:T(1024)S(1)} %get-tuple-element.59, f32[1408]{0:T(1024)S(1)} %get-tuple-element.58, f32[1408]{0:T(1024)S(1)} %get-tuple-element.57, ...), kind=kOutput, calls=%fused_computation.29 | convolution fusion | flops 5930745856 | bytes 21529600 | tf_op jit(solution)/shard_map/dot_general | solution.py:192
  572.9 28.2 %all_to_all.16 = bf16[2,512,2048]{2,1,0:T(8,128)(2,1)S(1)} all-to-all(bf16[2,512,2048]{2,1,0:T(8,128)(2,1)} %bitcast.82), channel_id=1, replica_groups=mesh['rep'=2,'fs'=32,'tp'=2] {'tp'}, dimensions={0} | all-to-all | bytes 8388608 | tf_op jit(solution)/shard_map/all_to_all | solution.py:50
  602.1 2.1 fusion.13
  (102 shorter events, 26.4 us)
Async XLA Ops:
  6.5 5.7 copy-start.7
  6.5 5.7 copy-start.8
  6.5 5.7 copy-start.9
  6.5 6.4 %copy-start.6 = (bf16[512,64]{0,1:T(8,128)(2,1)S(1)}, bf16[512,64]{0,1:T(8,128)(2,1)}, u32[]{:S(2)}) copy-start(bf16[512,64]{0,1:T(8,128)(2,1)} %param.19) | copy-start | bytes 196612
  6.5 25.8 %all-gather.7.cloned.1.call-start = ((), (), s32[]{:S(2)}) async-start(), calls=%async_computation.3 | async-start | bytes 6291456 | tf_op jit(solution)/shard_map/all_gather | solution.py:147
  12.2 160.4 %all-gather.9.cloned.1.call-start = ((), (), s32[]{:S(2)}) async-start(), calls=%async_computation.4 | async-start | bytes 4325376 | tf_op jit(solution)/shard_map/all_gather | solution.py:17
  14.6 193.9 %all-to-all-start = ((bf16[32,512,64]{1,2,0:T(8,128)(2,1)}), bf16[32,512,64]{1,2,0:T(8,128)(2,1)}, u32[]{:S(2)}, u32[]{:S(2)}) async-start(bf16[32,512,64]{1,2,0:T(8,128)(2,1)} %broadcast_in_dim.25), calls=%async_computation | async-start | bytes 4194304 | tf_op jit(solution)/shard_map/all_to_all | solution.py:26
  23.9 312.5 %all-gather.15.cloned.1.call-start = ((), (), s32[]{:S(2)}) async-start(), calls=%async_computation.7 | async-start | bytes 5947392 | tf_op jit(solution)/shard_map/all_gather | solution.py:190
  24.6 349.8 %all-gather.11.cloned.1.call-start = ((), (), s32[]{:S(2)}) async-start(), calls=%async_computation.5 | async-start | bytes 6291456 | tf_op jit(solution)/shard_map/all_gather | solution.py:175
  172.6 4.1 copy-start.12
  189.2 0.8 copy-start.1
  198.3 4.8 copy-start.2
  199.9 3.2 copy-start.3
  239.8 1.6 copy-start
  241.4 0.7 copy-start.10
  242.1 2.2 copy-start.4
  242.1 2.2 copy-start.5
  244.0 285.5 %all-gather.13.cloned.1.call-start = ((), (), s32[]{:S(2)}) async-start(), calls=%async_computation.6 | async-start | bytes 11894784 | tf_op jit(solution)/shard_map/all_gather | solution.py:17
  529.5 11.8 %copy-start.11 = (bf16[2048,2816]{1,0:T(8,128)(2,1)S(1)}, bf16[2048,2816]{1,0:T(8,128)(2,1)}, u32[]{:S(2)}) copy-start(bf16[2048,2816]{1,0:T(8,128)(2,1)} %all-gather.13.cloned.1.call-done) | copy-start | bytes 34603012
  529.6 11.8 %copy-start.13 = (bf16[1024,2048]{1,0:T(8,128)(2,1)S(1)}, bf16[1024,2048]{1,0:T(8,128)(2,1)}, u32[]{:S(2)}) copy-start(bf16[1024,2048]{1,0:T(8,128)(2,1)} %all-gather.11.cloned.1.call-done) | copy-start | bytes 12582916
Sparse Core Ops, SparseCore 0:
  12.3 19.9 all-gather.6
  34.0 138.5 all-gather.8
  174.2 162.1 all-gather.14
  338.0 36.4 all-gather.10
  376.0 153.5 all-gather.12
